TPU v7x, 512 devices: a whole 4x4x16 slice. The times are simulated.
512 devices in a mesh: ep: 128 (over z, x, core), tp: 4 (over y).
Axes of the slice: x: 4, y: 4, z: 16, core: 2. Of those that a mesh axis runs over, the one named last changes fastest.
Arguments:
- tokens: bfloat16 [16384, 2048], P('ep'), may hold values from -6 to 6
- norm_gain: float32 [2048], replicated, may hold values from 0.1 to 1.9
- expert_ids: int32 [16384, 2], P('ep'), may hold values from 0 to 31, all different within a row; in each aligned block of 128 rows (0 to 127, 128 to 255, ...) at most 12 rows name the same one
- gate_weights: float32 [16384, 2], P('ep'), may hold values from 0.2 to 1
- w_gate: bfloat16 [2048, 131072], P(None, ('ep', 'tp')), may hold values from -0.125 to 0.125
- w_up: bfloat16 [2048, 131072], P(None, ('ep', 'tp')), may hold values from -0.125 to 0.125
- w_down: bfloat16 [131072, 2048], P('ep', 'tp'), may hold values from -0.09375 to 0.09375
Outputs:
- moe_out: bfloat16 [16384, 2048], P('ep', 'tp')
Inputs may be any that keep to these rules, and one draw needn't show every extreme that they name: `expert_ids`: each token names 2 different experts; in each aligned block of 128 rows no expert is named by more than 12 rows, a bound that some block reaches.
All inputs are finite; a program needn't handle non-finite values.
Results may differ from a plain program's by a relative error of at most 0.0071.
Values may be sent and summed in bfloat16 or wider, within the bound.
A program may use at most 64 MiB of HBM per device.

v0:
```python
import jax
import jax.numpy as jnp
from jax import lax
from jax.sharding import Mesh
from jax.sharding import PartitionSpec as P

TOP = 2
EP = ("ep_0", "ep_1", "ep_2")
EP_TP = ("ep_0", "ep_1", "ep_2", "tp")


EPS = 1e-06


def split_up(array, dim, length):
    lengths = array.shape
    parts = array.reshape(*lengths[:dim], length, lengths[dim] // length, *lengths[dim + 1 :])
    return jnp.moveaxis(parts, dim, 0)


def laid_out(parts, dim):
    parts = jnp.moveaxis(parts, 0, dim)
    lengths = parts.shape
    return parts.reshape(*lengths[:dim], lengths[dim] * lengths[dim + 1], *lengths[dim + 2 :])


def turned_blocks(parts, axes, sequence):
    inside = parts.shape[1:]
    out = parts.reshape(*(lax.axis_size(a) for a in axes), *inside)
    for k in sequence:
        out = lax.all_to_all(out, axes[k], k, k, tiled=True)
    return out.reshape(-1, *inside)


def exchange_by_chip(array, groups, sequence, split_dim, concat_dim):
    length = lax.axis_size(groups[0]) * lax.axis_size(groups[1])
    parts = split_up(array, split_dim, length)
    return laid_out(turned_blocks(parts, groups, sequence), concat_dim)


def rms_rows(values, gain):
    widened = values.astype(jnp.float32)
    scale = lax.rsqrt(jnp.mean(widened * widened, axis=-1, keepdims=True) + EPS)
    return (widened * scale * gain).astype(jnp.bfloat16)


def on_device(tokens, norm_gain, expert_ids, gate_weights, w_gate, w_up, w_down):
    ep_count = lax.axis_size(EP)
    tp_count = lax.axis_size("tp")
    row_count = tokens.shape[0]
    group_size = max(1, ep_count // 32)
    expert_count = ep_count // group_size
    share = (row_count * TOP * 5 + 4 * expert_count * tp_count - 1) // (4 * expert_count * tp_count)
    capacity = min(row_count, tp_count * share)
    normed = rms_rows(tokens, norm_gain)
    flat_ids = expert_ids.reshape(-1)
    matches = (flat_ids[:, None] == jnp.arange(expert_count, dtype=jnp.int32)[None, :]).astype(
        jnp.int32
    )
    slot_index = jnp.sum((jnp.cumsum(matches, axis=0) - matches) * matches, axis=1)
    position = flat_ids * capacity + slot_index
    placing = (
        position[:, None] == jnp.arange(expert_count * capacity, dtype=jnp.int32)[None, :]
    ).astype(jnp.float32)
    placing = placing.reshape(row_count, TOP, expert_count * capacity)
    selector = jnp.sum(placing, axis=1).astype(jnp.bfloat16)
    buffers = lax.dot_general(
        selector, normed, (((0,), (0,)), ((), ())), preferred_element_type=jnp.float32
    )
    buffers = buffers.astype(jnp.bfloat16).reshape(expert_count, capacity, -1)
    quarter = capacity // tp_count
    mine = lax.dynamic_slice_in_dim(buffers, lax.axis_index("tp") * quarter, quarter, 1)
    copies = jnp.repeat(mine, group_size, axis=0)
    arrived = exchange_by_chip(copies, (("ep_0", "ep_1"), "ep_2"), (1, 0), 0, 0)
    received = lax.all_gather(arrived, "tp", axis=1, tiled=True)
    sources, slot_count, model_width = received.shape
    flat_rows = received.reshape(sources * slot_count, model_width)
    gate_proj = jnp.dot(flat_rows, w_gate, preferred_element_type=jnp.float32)
    upper = jnp.dot(flat_rows, w_up, preferred_element_type=jnp.float32)
    hidden = (jax.nn.silu(gate_proj) * upper).astype(jnp.bfloat16)
    partial_out = jnp.dot(
        lax.all_gather(hidden, "tp", axis=1, tiled=True), w_down, preferred_element_type=jnp.float32
    ).astype(jnp.bfloat16)
    partial_out = partial_out.reshape(sources, slot_count, w_down.shape[1])
    sources, slot_count, out_width = partial_out.shape
    back = exchange_by_chip(partial_out, (("ep_0", "ep_1"), "ep_2"), (1, 0), 0, 0)
    back = back.reshape(expert_count, group_size, slot_count, out_width).astype(jnp.float32)
    returned = jnp.sum(back, axis=1)
    summed = returned.reshape(expert_count * capacity, -1)
    combine = jnp.sum(placing * gate_weights[:, :, None], axis=1)
    mixed = jnp.dot(
        combine, summed, precision=lax.Precision.HIGHEST, preferred_element_type=jnp.float32
    )
    return mixed.astype(jnp.bfloat16)


def solution(mesh):
    finer = Mesh(mesh.devices.reshape(16, 4, 2, mesh.shape["tp"]), ("ep_0", "ep_1", "ep_2", "tp"))
    placed = (
        P(EP, None),
        P(),
        P(EP, None),
        P(EP, None),
        P(None, EP_TP),
        P(None, EP_TP),
        P(EP, "tp"),
    )
    return jax.shard_map(
        on_device, mesh=finer, in_specs=placed, out_specs=P(EP, "tp"), check_vma=False
    )
```

profile of v0, /device:TPU:1, one launch (start us, length us, event | category | flops | bytes accessed | tf_op | source)
XLA Modules:
  0.0 386.4 jit_solution(7729169001689056819)
XLA Ops:
  6.5 0.9 copy.81
  7.7 1.2 fusion.1
  11.7 1.4 convolution_convert_fusion.1
  13.1 1.5 reshape.57
  14.6 2.0 constant_dynamic-slice_fusion
  17.8 11.5 %all_to_all.20 = bf16[64,2,1,3,2048]{4,0,3,2,1:T(8,128)(2,1)S(1)} all-to-all(bf16[64,2,1,3,2048]{4,0,3,2,1:T(8,128)(2,1)S(1)} %broadcast_in_dim.15), channel_id=1, replica_groups=mesh['ep_0'=16,'ep_1'=4,'ep_2'=2,'tp'=4] {'ep_2'}, dimensions={1} | all-to-all | bytes 3145728 | tf_op jit(solution)/shard_map/all_to_all | solution.py:31
  29.3 1.6 copy.86
  30.9 86.5 %all_to_all.21 = bf16[64,2,1,3,2048]{4,1,3,2,0:T(2,128)(2,1)S(1)} all-to-all(bf16[64,2,1,3,2048]{4,1,3,2,0:T(2,128)(2,1)S(1)} %copy.86), channel_id=1, replica_groups=mesh['ep_0'=16,'ep_1'=4,'ep_2'=2,'tp'=4] {'ep_0','ep_1'}, dimensions={0} | all-to-all | bytes 3145728 | tf_op jit(solution)/shard_map/all_to_all | solution.py:31
  117.4 1.1 copy.87
  118.5 2.0 reshape_reshape.3
  120.8 69.1 %all-gather.3.cloned.1.call-done = bf16[128,12,2048]{2,0,1:T(8,128)(2,1)} async-done(((bf16[128,3,2048]{2,0,1:T(8,128)(2,1)}), bf16[128,12,2048]{2,0,1:T(8,128)(2,1)}) %all-gather.3.cloned.1.call-update) | async-done | bytes 6291472 | tf_op jit(solution)/shard_map/all_gather | solution.py:75
  190.0 9.7 %copy.88 = bf16[128,12,2048]{2,1,0:T(8,128)(2,1)} copy(bf16[128,12,2048]{2,0,1:T(8,128)(2,1)} %all-gather.3.cloned.1.call-done) | data formatting | bytes 12582912 | tf_op jit(solution)/shard_map/all_gather | solution.py:75
  199.6 10.8 %reshape.58 = bf16[1536,2048]{1,0:T(8,128)(2,1)} reshape(bf16[128,12,2048]{2,1,0:T(8,128)(2,1)} %copy.88) | data formatting | bytes 12582912 | tf_op jit(solution)/shard_map/reshape | solution.py:77
  210.4 4.8 %fusion.12 = f32[1536,256]{1,0:T(8,128)S(1)} fusion(bf16[1536,2048]{1,0:T(8,128)(2,1)} %reshape.58, bf16[2048,256]{1,0:T(8,128)(2,1)S(1)} %copy-done.3), kind=kOutput, calls=%fused_computation.30 | convolution fusion | flops 1610612736 | bytes 8912896 | tf_op jit(solution)/shard_map/dot_general | solution.py:78
  215.3 3.0 fusion
  218.2 50.0 %all-gather.5.cloned.1.call-done = bf16[1536,1024]{1,0:T(8,128)(2,1)} async-done(((bf16[1536,256]{1,0:T(8,128)(2,1)}), bf16[1536,1024]{1,0:T(8,128)(2,1)}) %all-gather.5.cloned.1.call-update) | async-done | bytes 3145744 | tf_op jit(solution)/shard_map/all_gather | solution.py:82
  268.3 4.8 %convolution_convert_fusion = bf16[1536,512]{1,0:T(8,128)(2,1)} fusion(bf16[1536,1024]{1,0:T(8,128)(2,1)} %all-gather.5.cloned.1.call-done, bf16[1024,512]{1,0:T(8,128)(2,1)S(1)} %copy-done), kind=kOutput, calls=%fused_computation.1 | convolution fusion | flops 1611399168 | bytes 5767168 | tf_op jit(solution)/shard_map/dot_general | solution.py:81
  273.1 2.4 reshape_reshape_reshape.2
  275.5 0.9 copy.89
  276.3 6.7 %all_to_all.22 = bf16[64,2,1,12,512]{4,0,3,2,1:T(8,128)(2,1)S(1)} all-to-all(bf16[64,2,1,12,512]{4,0,3,2,1:T(8,128)(2,1)S(1)} %copy.89), channel_id=1, replica_groups=mesh['ep_0'=16,'ep_1'=4,'ep_2'=2,'tp'=4] {'ep_2'}, dimensions={1} | all-to-all | bytes 3145728 | tf_op jit(solution)/shard_map/all_to_all | solution.py:31
  283.0 1.6 copy.90
  284.6 89.1 %all_to_all.23 = bf16[64,2,1,12,512]{4,1,3,2,0:T(2,128)(2,1)S(1)} all-to-all(bf16[64,2,1,12,512]{4,1,3,2,0:T(2,128)(2,1)S(1)} %copy.90), channel_id=1, replica_groups=mesh['ep_0'=16,'ep_1'=4,'ep_2'=2,'tp'=4] {'ep_0','ep_1'}, dimensions={0} | all-to-all | bytes 3145728 | tf_op jit(solution)/shard_map/all_to_all | solution.py:31
  373.7 4.2 %convert_reduce_fusion = f32[64,12,512]{2,1,0:T(8,128)S(1)} fusion(bf16[64,2,1,12,512]{4,1,3,2,0:T(2,128)(2,1)S(1)} %all_to_all.23), kind=kLoop, calls=%fused_computation | loop fusion | flops 1179648 | bytes 3145728 | tf_op jit(solution)/shard_map/reduce_sum | solution.py:88
  378.3 1.3 convolution_convert_fusion.2
  (33 shorter events, 4.8 us)
Async XLA Ops:
  6.5 261.7 %copy-start = (bf16[1024,512]{1,0:T(8,128)(2,1)S(1)}, bf16[1024,512]{1,0:T(8,128)(2,1)}, u32[]{:S(2)}) copy-start(bf16[1024,512]{1,0:T(8,128)(2,1)} %param.13) | copy-start | bytes 3145732
  6.5 5.1 %copy-start.2 = (bf16[128,2048]{1,0:T(8,128)(2,1)S(1)}, bf16[128,2048]{1,0:T(8,128)(2,1)}, u32[]{:S(2)}) copy-start(bf16[128,2048]{1,0:T(8,128)(2,1)} %param.7) | copy-start | bytes 1572868
  6.5 183.4 %all-gather.3.cloned.1.call-start = ((), (), s32[]{:S(2)}) async-start(), calls=%async_computation.4 | async-start | bytes 7864320 | tf_op jit(solution)/shard_map/all_gather | solution.py:75
  120.6 147.7 %all-gather.5.cloned.1.call-start = ((), (), s32[]{:S(2)}) async-start(), calls=%async_computation.5 | async-start | bytes 3932160 | tf_op jit(solution)/shard_map/all_gather | solution.py:82
  199.6 10.8 %copy-start.3 = (bf16[2048,256]{1,0:T(8,128)(2,1)S(1)}, bf16[2048,256]{1,0:T(8,128)(2,1)}, u32[]{:S(2)}) copy-start(bf16[2048,256]{1,0:T(8,128)(2,1)} %param.11) | copy-start | bytes 3145732
  210.4 4.8 %copy-start.1 = (bf16[1536,2048]{1,0:T(8,128)(2,1)S(1)}, bf16[1536,2048]{1,0:T(8,128)(2,1)}, u32[]{:S(2)}) copy-start(bf16[1536,2048]{1,0:T(8,128)(2,1)} %reshape.58) | copy-start | bytes 18874372
  210.4 4.9 %copy-start.4 = (bf16[2048,256]{1,0:T(8,128)(2,1)S(1)}, bf16[2048,256]{1,0:T(8,128)(2,1)}, u32[]{:S(2)}) copy-start(bf16[2048,256]{1,0:T(8,128)(2,1)} %param.12) | copy-start | bytes 3145732
Sparse Core Ops, SparseCore 0:
  120.7 69.2 all-gather.2
  218.4 49.8 all-gather.4
where the time goes:
time: 391 us; the launch traced here: 386 us
  blocking collectives  194 us (50%)
  waiting for transfers between devices  119 us (30%)
  local copies, waits for them, and re-layouts  36.5 us (9%)
  matrix products  15.2 us (4%)
  between operations  13.6 us (3%)
  other arithmetic  8.01 us (2%)
    all_to_all x4, blocking collectives, turned_blocks(): out = lax.all_to_all(out, axes[k], k, k, tiled=True)  194 us
    all_gather x1, waiting for transfers between devices, on_device(): received = lax.all_gather(arrived, 'tp', axis=1, tiled=True)  69.1 us
    all_gather x1, waiting for transfers between devices, on_device(): lax.all_gather(hidden, 'tp', axis=1, tiled=True)  50 us
    reshape x1, local copies, waits for them, and re-layouts, on_device(): flat_rows = received.reshape(sources * slot_count, model_width)  10.8 us
    all_gather x1, local copies, waits for them, and re-layouts, on_device(): received = lax.all_gather(arrived, 'tp', axis=1, tiled=True)  9.65 us
  transfers between devices with their start and end apart: 2, of which 2 were waited for; matrix products, arithmetic and copies ran while one was open for 0% of the time, Pallas kernels for 0%

commit v1 on v0

v1 whole, which is shorter than its diff:
```python
import functools

import jax
import jax.numpy as jnp
from jax import lax
from jax.experimental import pallas as pl
from jax.experimental.pallas import tpu as pltpu
from jax.sharding import Mesh
from jax.sharding import PartitionSpec as P

MESH = pl.DeviceIdType.MESH
EP = ("z", "x", "core")
EPS = 1e-06
XN = 4
CN = 2
YN = 4
K3 = 3
CAP = YN * K3
NEAR_FIRST = ((0, 1, -1, 2), (8, 7, -7, -6), (6, 5, -5, -4), (4, 3, -3, -2))

BF16 = jnp.bfloat16
F32 = jnp.float32


def chunks_of(zn):
    return NEAR_FIRST if zn == 16 else tuple((d,) for d in range(zn))


def when(stage, c):
    base = (5.0 * c, 5.0 * c + 3.0, 5.0 * c + 6.0, 8.3 * c + 12.0, 8.3 * c + 18.0, 8.3 * c + 22.0, 8.3 * c + 27.0)
    return base[stage]


def kernel(
    zn,
    tokens,
    gain,
    ids,
    gates,
    w_gate,
    w_up,
    w_down,
    out,
    sbuf,
    xb,
    fb,
    xr,
    hb,
    wgv,
    wuv,
    wdv,
    pf,
    pb,
    rsb,
    gb,
    rb,
    ret,
    vb,
    wl_sem,
    ws_sem,
    wr_sem,
    ds_sem,
    dr_sem,
    ys_sem,
    yr_sem,
    xs_sem,
    xr_sem,
    hs_sem,
    hr_sem,
    rs_sem,
    rr_sem,
    os_sem,
    or_sem,
):
    zc, xc, cc, yc = (lax.axis_index(a) for a in ("z", "x", "core", "tp"))
    chunks = chunks_of(zn)
    offsets = [d for chunk in chunks for d in chunk]
    messages = 2 * len(offsets)
    starts = [0]
    for chunk in chunks:
        starts.append(starts[-1] + 2 * len(chunk))
    row_count, width = tokens.shape
    pieces = width // 128
    units = w_gate.shape[1]
    out_pieces = w_down.shape[1] // 128

    other_x = XN - 1 - xc
    pair_x = xc + 1 - 2 * lax.rem(xc, 2)
    up_y, down_y = lax.rem(yc + 1, YN), lax.rem(yc + YN - 1, YN)
    sibling = (zc, xc, 1 - cc, yc)
    pair = (zc, pair_x, cc, yc)
    sides = ((zc, xc, cc, up_y), (zc, xc, cc, down_y))

    def far(m, sign):
        d = offsets[m // 2] * sign
        return (lax.rem(zc + d + zn, zn), xc if m % 2 == 0 else other_x, cc, yc)

    self_message = 2 * offsets.index(0)

    barrier = pltpu.get_barrier_semaphore()
    greeted = [far(m, 1) for m in range(messages) if m != self_message] + [sibling, pair, *sides]
    for device in greeted:
        pl.semaphore_signal(barrier, inc=1, device_id=device, device_id_type=MESH)

    weights = ((w_gate, wgv), (w_up, wuv), (w_down, wdv))
    own_weights = [pltpu.make_async_copy(src, dst.at[0], wl_sem.at[i]) for i, (src, dst) in enumerate(weights)]
    for copy in own_weights:
        copy.start()

    wide = tokens[...].astype(F32)
    scale = lax.rsqrt(jnp.mean(wide * wide, axis=-1, keepdims=True) + EPS)
    normed = (wide * scale * gain[...]).astype(BF16)

    earlier = (
        lax.broadcasted_iota(jnp.int32, (row_count, row_count), 1)
        < lax.broadcasted_iota(jnp.int32, (row_count, row_count), 0)
    ).astype(F32).astype(BF16)
    first_id, second_id = ids[:, 0:1], ids[:, 1:2]

    def expert_of(message):
        expert = jnp.zeros_like(message) - 1
        for m in range(messages):
            z, x, _, _ = far(m, 1)
            expert = jnp.where(message == m, z * (XN // 2) + x // 2, expert)
        return expert

    def selection(message, slot):
        expert = expert_of(message)
        hit_first, hit_second = first_id == expert, second_id == expert
        hit = jnp.where(hit_first | hit_second, 1.0, 0.0)
        rank = jnp.dot(earlier, hit.astype(BF16), preferred_element_type=F32)
        taken = jnp.where(rank == slot.astype(F32), hit, 0.0)
        return taken, hit_first

    lane = lax.broadcasted_iota(jnp.int32, (1, 128), 1)
    taken, _ = selection(lane // K3, K3 * yc + lane % K3)
    sent_rows = messages * K3
    placed = jnp.dot(jnp.transpose(taken).astype(BF16), normed, preferred_element_type=F32)
    for i in range(pieces):
        fb[pl.ds(i, sent_rows, stride=pieces), :] = placed[:sent_rows, i * 128 : (i + 1) * 128]
    sbuf[...] = fb[0 : sent_rows * pieces, :].reshape(sent_rows, pieces, 128).astype(BF16)
    xb[0, yc, self_message * K3 : (self_message + 1) * K3] = sbuf[self_message * K3 : (self_message + 1) * K3]

    pl.semaphore_wait(barrier, len(greeted))

    sends = []

    def remote(src, dst, send_sem, recv_sem, device, later=True):
        copy = pltpu.make_async_remote_copy(
            src_ref=src, dst_ref=dst, send_sem=send_sem, recv_sem=recv_sem, device_id=device, device_id_type=MESH
        )
        copy.start()
        if later:
            sends.append(copy)
        return copy

    def arrived(ref, sem):
        pltpu.make_async_copy(ref, ref, sem).wait()

    def without_self(c):
        m0, m1 = starts[c], starts[c + 1]
        if not m0 <= self_message < m1:
            return (m0, m1)
        assert self_message == m0
        return (m0 + 1, m1)

    for c in range(len(chunks)):
        for m in range(*without_self(c)):
            rows = pl.ds(m * K3, K3)
            remote(sbuf.at[rows], xb.at[0, yc, rows], ds_sem.at[c], dr_sem.at[c], far(m, 1), later=False)
    shared_weights = [
        remote(src, dst.at[1], ws_sem.at[i], wr_sem.at[i], sibling) for i, (src, dst) in enumerate(weights)
    ]

    lane = lax.broadcasted_iota(jnp.int32, (1, messages * CAP), 1)
    taken, hit_first = selection(lane // CAP, lane % CAP)
    mix = taken * jnp.where(hit_first, gates[:, 0:1], gates[:, 1:2])

    def run(c):
        m0, m1 = starts[c], starts[c + 1]
        return pl.ds(m0 * K3, (m1 - m0) * K3)

    def half(c, side):
        m0, m1 = starts[c], starts[c + 1]
        count = (m1 - m0) // 2 * K3
        return pl.ds(m0 * K3 + side * count, count)

    origin = [lax.rem(yc - r + YN, YN) for r in range(YN)]
    handles = {}

    def own_rows(c):
        m0, m1 = without_self(c)
        rows = pl.ds(m0 * K3, (m1 - m0) * K3)
        arrived(xb.at[0, yc, rows], dr_sem.at[c])
        block = xb.at[0, yc, run(c)]
        for side in (0, 1):
            handles["y", c, side] = remote(
                block, block, ys_sem.at[c, side], yr_sem.at[c, side], sides[side]
            )
        handles["x", c, 0] = remote(block, xb.at[1, yc, run(c)], xs_sem.at[c, 0], xr_sem.at[c, 0], pair)

    def next_rows(c):
        for side in (0, 1):
            handles["y", c, side].wait_recv()
            rel = 1 + 2 * side
            part = xb.at[0, origin[rel], half(c, side)]
            handles["f", c, side] = remote(
                part,
                part,
                ys_sem.at[c, 2 + side],
                yr_sem.at[c, 2 + side],
                sides[side],
            )
            handles["x", c, rel] = remote(
                xb.at[0, origin[rel], run(c)],
                xb.at[1, origin[rel], run(c)],
                xs_sem.at[c, rel],
                xr_sem.at[c, rel],
                pair,
            )

    def last_rows(c):
        for side in (0, 1):
            handles["f", c, side].wait_recv()
        handles["x", c, 2] = remote(
            xb.at[0, origin[2], run(c)], xb.at[1, origin[2], run(c)], xs_sem.at[c, 2], xr_sem.at[c, 2], pair
        )

    def chunk_rows(c):
        count = 2 * CAP * (starts[c + 1] - starts[c])
        return 2 * CAP * starts[c], count

    def first_product(c):
        for rel in range(YN):
            handles["x", c, rel].wait_recv()
        if c == 0:
            for copy in own_weights:
                copy.wait()
            for copy in shared_weights:
                copy.wait_recv()
        r0, count = chunk_rows(c)
        m0, m1 = starts[c], starts[c + 1]
        for side in (0, 1):
            for m in range(m0, m1):
                for y in range(YN):
                    at = ((side * (m1 - m0) + m - m0) * CAP + y * K3) * pieces
                    block = xb[side, y, m * K3 : (m + 1) * K3].astype(F32)
                    fb[at : at + K3 * pieces, :] = block.reshape(K3 * pieces, 128)
        for i in range(pieces):
            xr[0:count, i * 128 : (i + 1) * 128] = fb[pl.ds(i, count, stride=pieces), :].astype(BF16)
        for core in range(CN):
            gate = jnp.dot(xr[0:count, :], wgv[core], preferred_element_type=F32)
            upper = jnp.dot(xr[0:count, :], wuv[core], preferred_element_type=F32)
            hidden = gate / (1.0 + jnp.exp(-gate)) * upper
            hb[0, r0 : r0 + count, core * units : (core + 1) * units] = hidden.astype(BF16)
        for side in (0, 1):
            handles["h", c, side] = remote(
                hb.at[0, pl.ds(r0, count)],
                hb.at[1 + 2 * side, pl.ds(r0, count)],
                hs_sem.at[c, side],
                hr_sem.at[c, side],
                sides[side],
            )

    def next_hidden(c):
        r0, count = chunk_rows(c)
        for side in (0, 1):
            handles["h", c, side].wait_recv()
            rows = pl.ds(r0 + side * (count // 2), count // 2)
            handles["k", c, side] = remote(
                hb.at[1 + 2 * side, rows],
                hb.at[2, rows],
                hs_sem.at[c, 2 + side],
                hr_sem.at[c, 2 + side],
                sides[side],
            )

    def second_product(c):
        for side in (0, 1):
            handles["k", c, side].wait_recv()
        r0, count = chunk_rows(c)
        total = None
        for rel in range(YN):
            first = pl.multiple_of(origin[rel] * units, units)
            for core in range(CN):
                term = jnp.dot(
                    hb[rel, r0 : r0 + count, core * units : (core + 1) * units],
                    wdv[core, pl.ds(first, units), :],
                    preferred_element_type=F32,
                )
                total = term if total is None else total + term
        at, part = r0 // 2, count // 2
        pf[at : at + part, :] = total[0:part]
        pb[at : at + part, :] = total[part:count].astype(BF16)
        handles["r", c] = remote(
            pb.at[pl.ds(at, part)], rsb.at[pl.ds(at, part)], rs_sem.at[c], rr_sem.at[c], pair
        )

    def give_back(c):
        handles["r", c].wait_recv()
        r0, count = chunk_rows(c)
        at, part = r0 // 2, count // 2
        total = pf[at : at + part, :] + rsb[at : at + part, :].astype(F32)
        for i in range(out_pieces):
            gb[pl.ds(i, part, stride=out_pieces), :] = total[:, i * 128 : (i + 1) * 128]
        rb[at * out_pieces : (at + part) * out_pieces, :] = gb[0 : part * out_pieces, :].astype(BF16)
        size = CAP * out_pieces
        m0, m1 = starts[c], starts[c + 1]
        if m0 <= self_message < m1:
            ret[self_message * size : (self_message + 1) * size, :] = rb[
                self_message * size : (self_message + 1) * size, :
            ]
        for m in range(*without_self(c)):
            rows = pl.ds(m * size, size)
            remote(rb.at[rows], ret.at[rows], os_sem.at[c], or_sem.at[c], far(m, -1), later=False)

    stages = (own_rows, next_rows, last_rows, first_product, next_hidden, second_product, give_back)
    order = sorted((when(s, c), c, s) for c in range(len(chunks)) for s in range(len(stages)))
    for _, c, s in order:
        stages[s](c)

    size = CAP * out_pieces
    for c in range(len(chunks)):
        m0, m1 = without_self(c)
        arrived(ret.at[pl.ds(m0 * size, (m1 - m0) * size)], or_sem.at[c])
    gb[0 : messages * size, :] = ret[...].astype(F32)
    for i in range(out_pieces):
        vb[:, i * 128 : (i + 1) * 128] = gb[pl.ds(i, messages * CAP, stride=out_pieces), :].astype(BF16)
    values = vb[...]
    high = mix.astype(BF16)
    rest = mix - high.astype(F32)
    middle = rest.astype(BF16)
    low = (rest - middle.astype(F32)).astype(BF16)
    mixed = jnp.dot(high, values, preferred_element_type=F32)
    mixed = mixed + jnp.dot(middle, values, preferred_element_type=F32)
    mixed = mixed + jnp.dot(low, values, preferred_element_type=F32)
    out[...] = mixed.astype(BF16)

    for copy in sends:
        copy.wait_send()
    for c in range(len(chunks)):
        m0, m1 = without_self(c)
        arrived(sbuf.at[pl.ds(m0 * K3, (m1 - m0) * K3)], ds_sem.at[c])
        arrived(rb.at[pl.ds(m0 * size, (m1 - m0) * size)], os_sem.at[c])


def on_device(zn, tokens, norm_gain, expert_ids, gate_weights, w_gate, w_up, w_down):
    chunks = chunks_of(zn)
    n = len(chunks)
    messages = 2 * sum(len(chunk) for chunk in chunks)
    most = 2 * max(len(chunk) for chunk in chunks)
    row_count, width = tokens.shape
    pieces = width // 128
    units = w_gate.shape[1]
    block, columns = w_down.shape
    out_pieces = columns // 128
    rows = messages * CAP
    dma = pltpu.SemaphoreType.DMA
    scratch = [
        pltpu.VMEM((messages * K3, pieces, 128), BF16),
        pltpu.VMEM((2, YN, messages * K3, pieces, 128), BF16),
        pltpu.VMEM((max(2 * most * CAP, messages * K3) * pieces, 128), F32),
        pltpu.VMEM((2 * most * CAP, width), BF16),
        pltpu.VMEM((YN, 2 * rows, CN * units), BF16),
        pltpu.VMEM((CN, width, units), BF16),
        pltpu.VMEM((CN, width, units), BF16),
        pltpu.VMEM((CN, block, columns), BF16),
        pltpu.VMEM((rows, columns), F32),
        pltpu.VMEM((rows, columns), BF16),
        pltpu.VMEM((rows, columns), BF16),
        pltpu.VMEM((rows * out_pieces, 128), F32),
        pltpu.VMEM((rows * out_pieces, 128), BF16),
        pltpu.VMEM((rows * out_pieces, 128), BF16),
        pltpu.VMEM((rows, columns), BF16),
        dma((3,)),
        dma((3,)),
        dma((3,)),
        dma((n,)),
        dma((n,)),
        dma((n, 4)),
        dma((n, 4)),
        dma((n, 4)),
        dma((n, 4)),
        dma((n, 4)),
        dma((n, 4)),
        dma((n,)),
        dma((n,)),
        dma((n,)),
        dma((n,)),
    ]
    vmem = pl.BlockSpec(memory_space=pltpu.VMEM)
    hbm = pl.BlockSpec(memory_space=pl.ANY)
    return pl.pallas_call(
        functools.partial(kernel, zn),
        out_shape=jax.ShapeDtypeStruct((row_count, columns), BF16),
        in_specs=[vmem, vmem, vmem, vmem, hbm, hbm, hbm],
        out_specs=vmem,
        scratch_shapes=scratch,
        compiler_params=pltpu.CompilerParams(
            collective_id=0, has_side_effects=True, vmem_limit_bytes=60 * 1024 * 1024
        ),
        name="expert_layer",
    )(tokens, norm_gain.reshape(1, width), expert_ids, gate_weights, w_gate, w_up, w_down)


def solution(mesh):
    zn = mesh.shape["ep"] // (XN * CN)
    finer = Mesh(mesh.devices.reshape(zn, XN, CN, mesh.shape["tp"]), (*EP, "tp"))
    placed = (
        P(EP, None),
        P(),
        P(EP, None),
        P(EP, None),
        P(None, (*EP, "tp")),
        P(None, (*EP, "tp")),
        P(EP, "tp"),
    )
    return jax.shard_map(
        functools.partial(on_device, zn), mesh=finer, in_specs=placed, out_specs=P(EP, "tp"), check_vma=False
    )
```

time: 391 us -> 99.8 us (0.26)
  the two profiles are of different devices: /device:TPU:1 before, /device:TPU:8 now
where the time goes in v1:
time: 99.8 us; the launch traced here: 99.6 us
  Pallas kernels  95.9 us (96%)
  local copies, waits for them, and re-layouts  3.72 us (4%)
    pallas_call x1, Pallas kernels, on_device(): pl.pallas_call(functools.partial(kernel, zn), out_shape=jax.ShapeDtypeStr...  95.9 us
    unnamed x7, local copies, waits for them, and re-layouts  3.72 us

profile of v1, /device:TPU:8, one launch (start us, length us, event | category | flops | bytes accessed | tf_op | source)
XLA Modules:
  0.0 99.6 jit_solution(10344748926305165300)
XLA Ops:
  0.0 0.0 copy-start
  0.0 0.7 copy-done
  0.7 0.0 copy-start.1
  0.7 0.7 copy.8.ids
  1.4 0.0 copy-done.1
  1.4 0.7 copy.9.gates
  2.2 95.9 %expert_layer.1 = bf16[128,512]{1,0:T(8,128)(2,1)} custom-call(bf16[128,2048]{1,0:T(8,128)(2,1)} %tokens.1, f32[1,2048]{1,0:T(1,128)} %bitcast.1, s32[128,2]{1,0:T(8,128)} %copy.8.ids, f32[128,2]{1,0:T(8,128)} %copy.9.gates, bf16[2048,256]{1,0:T(8,128)(2,1)} %w_gate.1, bf16[2048,256]{1,0:T(8,128)(2,1)} %w_up.1, bf16[1024,512]{1,0:T(8,128)(2,1)} %w_down.1), custom_call_target="tpu_custom_call" | custom-call | tf_op jit(solution)/shard_map/expert_layer/pallas_call | solution.py:393
  98.0 1.6 %copy.11 = bf16[128,512]{1,0:T(8,128)(2,1)} copy(bf16[128,512]{1,0:T(8,128)(2,1)} %expert_layer.1) | data formatting | bytes 262144
Async XLA Ops:
  0.0 0.7 copy-start
  0.7 0.7 copy-start.1

commit v2 on v1

--- a/solution.py
+++ b/solution.py
@@ -16,24 +16,24 @@
 YN = 4
 K3 = 3
 CAP = YN * K3
-NEAR_FIRST = ((0, 1, -1, 2), (8, 7, -7, -6), (6, 5, -5, -4), (4, 3, -3, -2))
+CHUNKS = ((-1, 1), (5, -5), (6, -6), (2, -2), (-7, 7), (8, 0), (-4, 4), (-3, 3))
+ORDER = "00101312032412641352460762541325746132754673405637567570"
 
 BF16 = jnp.bfloat16
 F32 = jnp.float32
 
 
 def chunks_of(zn):
-    return NEAR_FIRST if zn == 16 else tuple((d,) for d in range(zn))
-
-
-def when(stage, c):
-    base = (5.0 * c, 5.0 * c + 3.0, 5.0 * c + 6.0, 8.3 * c + 12.0, 8.3 * c + 18.0, 8.3 * c + 22.0, 8.3 * c + 27.0)
-    return base[stage]
+    return CHUNKS if zn == 16 else tuple((d,) for d in range(zn))
+
+
+def order_of(count):
+    return [int(c) for c in ORDER] if count == 8 else [c for c in range(count) for _ in range(7)]
 
 
 def kernel(
     zn,
-    tokens,
+    tokens_hbm,
     gain,
     ids,
     gates,
@@ -41,6 +41,8 @@
     w_up,
     w_down,
     out,
+    tokens,
+    t_sem,
     sbuf,
     xb,
     fb,
@@ -79,7 +81,7 @@
     starts = [0]
     for chunk in chunks:
         starts.append(starts[-1] + 2 * len(chunk))
-    row_count, width = tokens.shape
+    row_count, width = tokens_hbm.shape
     pieces = width // 128
     units = w_gate.shape[1]
     out_pieces = w_down.shape[1] // 128
@@ -93,12 +95,12 @@
 
     def far(m, sign):
         d = offsets[m // 2] * sign
-        return (lax.rem(zc + d + zn, zn), xc if m % 2 == 0 else other_x, cc, yc)
-
-    self_message = 2 * offsets.index(0)
-
+        return (lax.rem(zc + d + zn, zn), xc if m % 2 == 0 else other_x, 1 - cc, yc)
+
+    token_copy = pltpu.make_async_copy(tokens_hbm, tokens, t_sem)
+    token_copy.start()
     barrier = pltpu.get_barrier_semaphore()
-    greeted = [far(m, 1) for m in range(messages) if m != self_message] + [sibling, pair, *sides]
+    greeted = [far(m, 1) for m in range(messages)] + [pair, *sides]
     for device in greeted:
         pl.semaphore_signal(barrier, inc=1, device_id=device, device_id_type=MESH)
 
@@ -107,15 +109,17 @@
     for copy in own_weights:
         copy.start()
 
+    token_copy.wait()
     wide = tokens[...].astype(F32)
     scale = lax.rsqrt(jnp.mean(wide * wide, axis=-1, keepdims=True) + EPS)
     normed = (wide * scale * gain[...]).astype(BF16)
 
     earlier = (
-        lax.broadcasted_iota(jnp.int32, (row_count, row_count), 1)
-        < lax.broadcasted_iota(jnp.int32, (row_count, row_count), 0)
-    ).astype(F32).astype(BF16)
-    first_id, second_id = ids[:, 0:1], ids[:, 1:2]
+        lax.broadcasted_iota(jnp.int32, (row_count, row_count), 0)
+        < lax.broadcasted_iota(jnp.int32, (row_count, row_count), 1)
+    )
+    earlier = jnp.where(earlier, 1.0, 0.0).astype(BF16)
+    first_id, second_id = ids[0:1, :], ids[1:2, :]
 
     def expert_of(message):
         expert = jnp.zeros_like(message) - 1
@@ -128,18 +132,17 @@
         expert = expert_of(message)
         hit_first, hit_second = first_id == expert, second_id == expert
         hit = jnp.where(hit_first | hit_second, 1.0, 0.0)
-        rank = jnp.dot(earlier, hit.astype(BF16), preferred_element_type=F32)
+        rank = jnp.dot(hit.astype(BF16), earlier, preferred_element_type=F32)
         taken = jnp.where(rank == slot.astype(F32), hit, 0.0)
         return taken, hit_first
 
-    lane = lax.broadcasted_iota(jnp.int32, (1, 128), 1)
-    taken, _ = selection(lane // K3, K3 * yc + lane % K3)
+    line = lax.broadcasted_iota(jnp.int32, (128, 1), 0)
+    taken, _ = selection(line // K3, K3 * yc + line % K3)
     sent_rows = messages * K3
-    placed = jnp.dot(jnp.transpose(taken).astype(BF16), normed, preferred_element_type=F32)
+    placed = jnp.dot(taken.astype(BF16), normed, preferred_element_type=F32)
     for i in range(pieces):
         fb[pl.ds(i, sent_rows, stride=pieces), :] = placed[:sent_rows, i * 128 : (i + 1) * 128]
     sbuf[...] = fb[0 : sent_rows * pieces, :].reshape(sent_rows, pieces, 128).astype(BF16)
-    xb[0, yc, self_message * K3 : (self_message + 1) * K3] = sbuf[self_message * K3 : (self_message + 1) * K3]
 
     pl.semaphore_wait(barrier, len(greeted))
 
@@ -157,24 +160,17 @@
     def arrived(ref, sem):
         pltpu.make_async_copy(ref, ref, sem).wait()
 
-    def without_self(c):
-        m0, m1 = starts[c], starts[c + 1]
-        if not m0 <= self_message < m1:
-            return (m0, m1)
-        assert self_message == m0
-        return (m0 + 1, m1)
-
     for c in range(len(chunks)):
-        for m in range(*without_self(c)):
+        for m in range(starts[c], starts[c + 1]):
             rows = pl.ds(m * K3, K3)
             remote(sbuf.at[rows], xb.at[0, yc, rows], ds_sem.at[c], dr_sem.at[c], far(m, 1), later=False)
     shared_weights = [
         remote(src, dst.at[1], ws_sem.at[i], wr_sem.at[i], sibling) for i, (src, dst) in enumerate(weights)
     ]
 
-    lane = lax.broadcasted_iota(jnp.int32, (1, messages * CAP), 1)
-    taken, hit_first = selection(lane // CAP, lane % CAP)
-    mix = taken * jnp.where(hit_first, gates[:, 0:1], gates[:, 1:2])
+    line = lax.broadcasted_iota(jnp.int32, (messages * CAP, 1), 0)
+    taken, hit_first = selection(line // CAP, line % CAP)
+    mix = jnp.transpose(taken * jnp.where(hit_first, gates[0:1, :], gates[1:2, :]))
 
     def run(c):
         m0, m1 = starts[c], starts[c + 1]
@@ -189,10 +185,8 @@
     handles = {}
 
     def own_rows(c):
-        m0, m1 = without_self(c)
-        rows = pl.ds(m0 * K3, (m1 - m0) * K3)
-        arrived(xb.at[0, yc, rows], dr_sem.at[c])
         block = xb.at[0, yc, run(c)]
+        arrived(block, dr_sem.at[c])
         for side in (0, 1):
             handles["y", c, side] = remote(
                 block, block, ys_sem.at[c, side], yr_sem.at[c, side], sides[side]
@@ -233,7 +227,8 @@
     def first_product(c):
         for rel in range(YN):
             handles["x", c, rel].wait_recv()
-        if c == 0:
+        if not handles.get("weights"):
+            handles["weights"] = True
             for copy in own_weights:
                 copy.wait()
             for copy in shared_weights:
@@ -305,23 +300,19 @@
             gb[pl.ds(i, part, stride=out_pieces), :] = total[:, i * 128 : (i + 1) * 128]
         rb[at * out_pieces : (at + part) * out_pieces, :] = gb[0 : part * out_pieces, :].astype(BF16)
         size = CAP * out_pieces
-        m0, m1 = starts[c], starts[c + 1]
-        if m0 <= self_message < m1:
-            ret[self_message * size : (self_message + 1) * size, :] = rb[
-                self_message * size : (self_message + 1) * size, :
-            ]
-        for m in range(*without_self(c)):
+        for m in range(starts[c], starts[c + 1]):
             rows = pl.ds(m * size, size)
             remote(rb.at[rows], ret.at[rows], os_sem.at[c], or_sem.at[c], far(m, -1), later=False)
 
     stages = (own_rows, next_rows, last_rows, first_product, next_hidden, second_product, give_back)
-    order = sorted((when(s, c), c, s) for c in range(len(chunks)) for s in range(len(stages)))
-    for _, c, s in order:
-        stages[s](c)
+    reached = [0] * len(chunks)
+    for c in order_of(len(chunks)):
+        stages[reached[c]](c)
+        reached[c] += 1
 
     size = CAP * out_pieces
     for c in range(len(chunks)):
-        m0, m1 = without_self(c)
+        m0, m1 = starts[c], starts[c + 1]
         arrived(ret.at[pl.ds(m0 * size, (m1 - m0) * size)], or_sem.at[c])
     gb[0 : messages * size, :] = ret[...].astype(F32)
     for i in range(out_pieces):
@@ -339,7 +330,7 @@
     for copy in sends:
         copy.wait_send()
     for c in range(len(chunks)):
-        m0, m1 = without_self(c)
+        m0, m1 = starts[c], starts[c + 1]
         arrived(sbuf.at[pl.ds(m0 * K3, (m1 - m0) * K3)], ds_sem.at[c])
         arrived(rb.at[pl.ds(m0 * size, (m1 - m0) * size)], os_sem.at[c])
 
@@ -357,6 +348,8 @@
     rows = messages * CAP
     dma = pltpu.SemaphoreType.DMA
     scratch = [
+        pltpu.VMEM((row_count, width), BF16),
+        dma(()),
         pltpu.VMEM((messages * K3, pieces, 128), BF16),
         pltpu.VMEM((2, YN, messages * K3, pieces, 128), BF16),
         pltpu.VMEM((max(2 * most * CAP, messages * K3) * pieces, 128), F32),
@@ -393,14 +386,14 @@
     return pl.pallas_call(
         functools.partial(kernel, zn),
         out_shape=jax.ShapeDtypeStruct((row_count, columns), BF16),
-        in_specs=[vmem, vmem, vmem, vmem, hbm, hbm, hbm],
+        in_specs=[hbm, vmem, vmem, vmem, hbm, hbm, hbm],
         out_specs=vmem,
         scratch_shapes=scratch,
         compiler_params=pltpu.CompilerParams(
             collective_id=0, has_side_effects=True, vmem_limit_bytes=60 * 1024 * 1024
         ),
         name="expert_layer",
-    )(tokens, norm_gain.reshape(1, width), expert_ids, gate_weights, w_gate, w_up, w_down)
+    )(tokens, norm_gain.reshape(1, width), expert_ids.T, gate_weights.T, w_gate, w_up, w_down)
 
 
 def solution(mesh):

time: 99.8 us -> 89 us (0.89)
  the two profiles are of different devices: /device:TPU:8 before, /device:TPU:1 now
where the time goes in v2:
time: 89 us; the launch traced here: 88.9 us
  Pallas kernels  87.3 us (98%)
  local copies, waits for them, and re-layouts  1.57 us (2%)
    pallas_call x1, Pallas kernels, on_device(): pl.pallas_call(functools.partial(kernel, zn), out_shape=jax.ShapeDtypeStr...  87.3 us

profile of v2, /device:TPU:1, one launch (start us, length us, event | category | flops | bytes accessed | tf_op | source)
XLA Modules:
  0.0 88.9 jit_solution(12577011486102073310)
XLA Ops:
  0.0 87.3 %expert_layer.1 = bf16[128,512]{1,0:T(8,128)(2,1)} custom-call(bf16[128,2048]{1,0:T(8,128)(2,1)} %tokens_hbm.1, f32[1,2048]{1,0:T(1,128)} %bitcast.3, s32[2,128]{1,0:T(2,128)} %bitcast.4, f32[2,128]{1,0:T(2,128)} %bitcast.5, bf16[2048,256]{1,0:T(8,128)(2,1)} %w_gate.1, bf16[2048,256]{1,0:T(8,128)(2,1)} %w_up.1, bf16[1024,512]{1,0:T(8,128)(2,1)} %w_down.1), custom_call_target="tpu_custom_call" | custom-call | tf_op jit(solution)/shard_map/expert_layer/pallas_call | solution.py:386
  87.3 1.6 %copy.9 = bf16[128,512]{1,0:T(8,128)(2,1)} copy(bf16[128,512]{1,0:T(8,128)(2,1)} %expert_layer.1) | data formatting | bytes 262144

commit v3 on v2

--- a/solution.py
+++ b/solution.py
@@ -16,8 +16,8 @@
 YN = 4
 K3 = 3
 CAP = YN * K3
-CHUNKS = ((-1, 1), (5, -5), (6, -6), (2, -2), (-7, 7), (8, 0), (-4, 4), (-3, 3))
-ORDER = "00101312032412641352460762541325746132754673405637567570"
+CHUNKS = ((2, -2), (4, -4), (8, 0), (1, -1), (7, -7), (-6, 6), (-5, 5), (-3, 3))
+ORDER = "01030121402451462057145062146752401735643275632756376373"
 
 BF16 = jnp.bfloat16
 F32 = jnp.float32
@@ -146,15 +146,11 @@
 
     pl.semaphore_wait(barrier, len(greeted))
 
-    sends = []
-
-    def remote(src, dst, send_sem, recv_sem, device, later=True):
+    def remote(src, dst, send_sem, recv_sem, device):
         copy = pltpu.make_async_remote_copy(
             src_ref=src, dst_ref=dst, send_sem=send_sem, recv_sem=recv_sem, device_id=device, device_id_type=MESH
         )
         copy.start()
-        if later:
-            sends.append(copy)
         return copy
 
     def arrived(ref, sem):
@@ -163,7 +159,7 @@
     for c in range(len(chunks)):
         for m in range(starts[c], starts[c + 1]):
             rows = pl.ds(m * K3, K3)
-            remote(sbuf.at[rows], xb.at[0, yc, rows], ds_sem.at[c], dr_sem.at[c], far(m, 1), later=False)
+            remote(sbuf.at[rows], xb.at[0, yc, rows], ds_sem, dr_sem.at[c], far(m, 1))
     shared_weights = [
         remote(src, dst.at[1], ws_sem.at[i], wr_sem.at[i], sibling) for i, (src, dst) in enumerate(weights)
     ]
@@ -189,9 +185,9 @@
         arrived(block, dr_sem.at[c])
         for side in (0, 1):
             handles["y", c, side] = remote(
-                block, block, ys_sem.at[c, side], yr_sem.at[c, side], sides[side]
+                block, block, ys_sem, yr_sem.at[c, side], sides[side]
             )
-        handles["x", c, 0] = remote(block, xb.at[1, yc, run(c)], xs_sem.at[c, 0], xr_sem.at[c, 0], pair)
+        handles["x", c, 0] = remote(block, xb.at[1, yc, run(c)], xs_sem, xr_sem.at[c], pair)
 
     def next_rows(c):
         for side in (0, 1):
@@ -201,23 +197,22 @@
             handles["f", c, side] = remote(
                 part,
                 part,
-                ys_sem.at[c, 2 + side],
-                yr_sem.at[c, 2 + side],
+                ys_sem,
+                yr_sem.at[c, 2],
                 sides[side],
             )
             handles["x", c, rel] = remote(
                 xb.at[0, origin[rel], run(c)],
                 xb.at[1, origin[rel], run(c)],
-                xs_sem.at[c, rel],
-                xr_sem.at[c, rel],
+                xs_sem,
+                xr_sem.at[c],
                 pair,
             )
 
     def last_rows(c):
-        for side in (0, 1):
-            handles["f", c, side].wait_recv()
+        arrived(xb.at[0, origin[2], run(c)], yr_sem.at[c, 2])
         handles["x", c, 2] = remote(
-            xb.at[0, origin[2], run(c)], xb.at[1, origin[2], run(c)], xs_sem.at[c, 2], xr_sem.at[c, 2], pair
+            xb.at[0, origin[2], run(c)], xb.at[1, origin[2], run(c)], xs_sem, xr_sem.at[c], pair
         )
 
     def chunk_rows(c):
@@ -225,8 +220,7 @@
         return 2 * CAP * starts[c], count
 
     def first_product(c):
-        for rel in range(YN):
-            handles["x", c, rel].wait_recv()
+        arrived(xb.at[1, :, run(c)], xr_sem.at[c])
         if not handles.get("weights"):
             handles["weights"] = True
             for copy in own_weights:
@@ -252,7 +246,7 @@
             handles["h", c, side] = remote(
                 hb.at[0, pl.ds(r0, count)],
                 hb.at[1 + 2 * side, pl.ds(r0, count)],
-                hs_sem.at[c, side],
+                hs_sem,
                 hr_sem.at[c, side],
                 sides[side],
             )
@@ -265,15 +259,14 @@
             handles["k", c, side] = remote(
                 hb.at[1 + 2 * side, rows],
                 hb.at[2, rows],
-                hs_sem.at[c, 2 + side],
-                hr_sem.at[c, 2 + side],
+                hs_sem,
+                hr_sem.at[c, 2],
                 sides[side],
             )
 
     def second_product(c):
-        for side in (0, 1):
-            handles["k", c, side].wait_recv()
         r0, count = chunk_rows(c)
+        arrived(hb.at[2, pl.ds(r0, count)], hr_sem.at[c, 2])
         total = None
         for rel in range(YN):
             first = pl.multiple_of(origin[rel] * units, units)
@@ -288,7 +281,7 @@
         pf[at : at + part, :] = total[0:part]
         pb[at : at + part, :] = total[part:count].astype(BF16)
         handles["r", c] = remote(
-            pb.at[pl.ds(at, part)], rsb.at[pl.ds(at, part)], rs_sem.at[c], rr_sem.at[c], pair
+            pb.at[pl.ds(at, part)], rsb.at[pl.ds(at, part)], rs_sem, rr_sem.at[c], pair
         )
 
     def give_back(c):
@@ -302,7 +295,7 @@
         size = CAP * out_pieces
         for m in range(starts[c], starts[c + 1]):
             rows = pl.ds(m * size, size)
-            remote(rb.at[rows], ret.at[rows], os_sem.at[c], or_sem.at[c], far(m, -1), later=False)
+            remote(rb.at[rows], ret.at[rows], os_sem, or_sem, far(m, -1))
 
     stages = (own_rows, next_rows, last_rows, first_product, next_hidden, second_product, give_back)
     reached = [0] * len(chunks)
@@ -311,9 +304,7 @@
         reached[c] += 1
 
     size = CAP * out_pieces
-    for c in range(len(chunks)):
-        m0, m1 = starts[c], starts[c + 1]
-        arrived(ret.at[pl.ds(m0 * size, (m1 - m0) * size)], or_sem.at[c])
+    arrived(ret, or_sem)
     gb[0 : messages * size, :] = ret[...].astype(F32)
     for i in range(out_pieces):
         vb[:, i * 128 : (i + 1) * 128] = gb[pl.ds(i, messages * CAP, stride=out_pieces), :].astype(BF16)
@@ -327,12 +318,18 @@
     mixed = mixed + jnp.dot(low, values, preferred_element_type=F32)
     out[...] = mixed.astype(BF16)
 
-    for copy in sends:
+    for copy in shared_weights:
         copy.wait_send()
-    for c in range(len(chunks)):
-        m0, m1 = starts[c], starts[c + 1]
-        arrived(sbuf.at[pl.ds(m0 * K3, (m1 - m0) * K3)], ds_sem.at[c])
-        arrived(rb.at[pl.ds(m0 * size, (m1 - m0) * size)], os_sem.at[c])
+    three = pl.ds(0, YN - 1)
+    for ref, sem in (
+        (sbuf, ds_sem),
+        (xb.at[0, three], ys_sem),
+        (xb.at[1], xs_sem),
+        (hb.at[three], hs_sem),
+        (pb, rs_sem),
+        (rb, os_sem),
+    ):
+        arrived(ref, sem)
 
 
 def on_device(zn, tokens, norm_gain, expert_ids, gate_weights, w_gate, w_up, w_down):
@@ -368,18 +365,18 @@
         dma((3,)),
         dma((3,)),
         dma((3,)),
+        dma(()),
         dma((n,)),
+        dma(()),
+        dma((n, 3)),
+        dma(()),
         dma((n,)),
-        dma((n, 4)),
-        dma((n, 4)),
-        dma((n, 4)),
-        dma((n, 4)),
-        dma((n, 4)),
-        dma((n, 4)),
+        dma(()),
+        dma((n, 3)),
+        dma(()),
         dma((n,)),
-        dma((n,)),
-        dma((n,)),
-        dma((n,)),
+        dma(()),
+        dma(()),
     ]
     vmem = pl.BlockSpec(memory_space=pltpu.VMEM)
     hbm = pl.BlockSpec(memory_space=pl.ANY)

time: 89 us -> 87.5 us (0.983)
  Pallas kernels: 87.3 us -> 85.7 us
    pallas_call x1, Pallas kernels: 87.3 us -> 85.7 us  [on_device(): pl.pallas_call(functools.partial(kernel, zn), out_shape=jax.ShapeDtypeStr...]
where the time goes in v3:
time: 87.5 us; the launch traced here: 87.3 us
  Pallas kernels  85.7 us (98%)
  local copies, waits for them, and re-layouts  1.57 us (2%)
    pallas_call x1, Pallas kernels, on_device(): pl.pallas_call(functools.partial(kernel, zn), out_shape=jax.ShapeDtypeStr...  85.7 us

profile of v3, /device:TPU:1, one launch (start us, length us, event | category | flops | bytes accessed | tf_op | source)
XLA Modules:
  0.0 87.3 jit_solution(17363977618378816614)
XLA Ops:
  0.0 85.7 %expert_layer.1 = bf16[128,512]{1,0:T(8,128)(2,1)} custom-call(bf16[128,2048]{1,0:T(8,128)(2,1)} %tokens_hbm.1, f32[1,2048]{1,0:T(1,128)} %bitcast.3, s32[2,128]{1,0:T(2,128)} %bitcast.4, f32[2,128]{1,0:T(2,128)} %bitcast.5, bf16[2048,256]{1,0:T(8,128)(2,1)} %w_gate.1, bf16[2048,256]{1,0:T(8,128)(2,1)} %w_up.1, bf16[1024,512]{1,0:T(8,128)(2,1)} %w_down.1), custom_call_target="tpu_custom_call" | custom-call | tf_op jit(solution)/shard_map/expert_layer/pallas_call | solution.py:383
  85.8 1.6 %copy.9 = bf16[128,512]{1,0:T(8,128)(2,1)} copy(bf16[128,512]{1,0:T(8,128)(2,1)} %expert_layer.1) | data formatting | bytes 262144

commit v4 on v3

--- a/solution.py
+++ b/solution.py
@@ -16,8 +16,8 @@
 YN = 4
 K3 = 3
 CAP = YN * K3
-CHUNKS = ((2, -2), (4, -4), (8, 0), (1, -1), (7, -7), (-6, 6), (-5, 5), (-3, 3))
-ORDER = "01030121402451462057145062146752401735643275632756376373"
+CHUNKS = ((2, -2), (-5, 5), (7, -7), (4, -4), (8, 0), (1, -1), (-6, 6), (-3, 3))
+ORDER = "00101213024312467124630254617325741603524670354673567575"
 
 BF16 = jnp.bfloat16
 F32 = jnp.float32
@@ -34,14 +34,17 @@
 def kernel(
     zn,
     tokens_hbm,
-    gain,
-    ids,
-    gates,
+    gain_hbm,
+    ids_hbm,
+    gates_hbm,
     w_gate,
     w_up,
     w_down,
     out,
     tokens,
+    gain,
+    ids,
+    gates,
     t_sem,
     sbuf,
     xb,
@@ -97,8 +100,10 @@
         d = offsets[m // 2] * sign
         return (lax.rem(zc + d + zn, zn), xc if m % 2 == 0 else other_x, 1 - cc, yc)
 
-    token_copy = pltpu.make_async_copy(tokens_hbm, tokens, t_sem)
-    token_copy.start()
+    small = ((tokens_hbm, tokens), (gain_hbm, gain), (ids_hbm, ids), (gates_hbm, gates))
+    inputs = [pltpu.make_async_copy(src, dst, t_sem.at[i]) for i, (src, dst) in enumerate(small)]
+    for copy in inputs:
+        copy.start()
     barrier = pltpu.get_barrier_semaphore()
     greeted = [far(m, 1) for m in range(messages)] + [pair, *sides]
     for device in greeted:
@@ -109,7 +114,8 @@
     for copy in own_weights:
         copy.start()
 
-    token_copy.wait()
+    for copy in inputs:
+        copy.wait()
     wide = tokens[...].astype(F32)
     scale = lax.rsqrt(jnp.mean(wide * wide, axis=-1, keepdims=True) + EPS)
     normed = (wide * scale * gain[...]).astype(BF16)
@@ -183,24 +189,21 @@
     def own_rows(c):
         block = xb.at[0, yc, run(c)]
         arrived(block, dr_sem.at[c])
-        for side in (0, 1):
-            handles["y", c, side] = remote(
-                block, block, ys_sem, yr_sem.at[c, side], sides[side]
-            )
+        for part in (0, 1):
+            for side in (0, 1):
+                rows = xb.at[0, yc, half(c, (side + part) % 2)]
+                handles["y", c, side, part] = remote(rows, rows, ys_sem, yr_sem.at[c, 2 * part + side], sides[side])
         handles["x", c, 0] = remote(block, xb.at[1, yc, run(c)], xs_sem, xr_sem.at[c], pair)
 
     def next_rows(c):
         for side in (0, 1):
-            handles["y", c, side].wait_recv()
             rel = 1 + 2 * side
             part = xb.at[0, origin[rel], half(c, side)]
-            handles["f", c, side] = remote(
-                part,
-                part,
-                ys_sem,
-                yr_sem.at[c, 2],
-                sides[side],
-            )
+            arrived(part, yr_sem.at[c, side])
+            remote(part, part, ys_sem, yr_sem.at[c, 4], sides[side])
+        for side in (0, 1):
+            rel = 1 + 2 * side
+            arrived(xb.at[0, origin[rel], half(c, 1 - side)], yr_sem.at[c, 2 + side])
             handles["x", c, rel] = remote(
                 xb.at[0, origin[rel], run(c)],
                 xb.at[1, origin[rel], run(c)],
@@ -210,7 +213,7 @@
             )
 
     def last_rows(c):
-        arrived(xb.at[0, origin[2], run(c)], yr_sem.at[c, 2])
+        arrived(xb.at[0, origin[2], run(c)], yr_sem.at[c, 4])
         handles["x", c, 2] = remote(
             xb.at[0, origin[2], run(c)], xb.at[1, origin[2], run(c)], xs_sem, xr_sem.at[c], pair
         )
@@ -241,38 +244,36 @@
             gate = jnp.dot(xr[0:count, :], wgv[core], preferred_element_type=F32)
             upper = jnp.dot(xr[0:count, :], wuv[core], preferred_element_type=F32)
             hidden = gate / (1.0 + jnp.exp(-gate)) * upper
-            hb[0, r0 : r0 + count, core * units : (core + 1) * units] = hidden.astype(BF16)
-        for side in (0, 1):
-            handles["h", c, side] = remote(
-                hb.at[0, pl.ds(r0, count)],
-                hb.at[1 + 2 * side, pl.ds(r0, count)],
-                hs_sem,
-                hr_sem.at[c, side],
-                sides[side],
-            )
+            hb[0, core, r0 : r0 + count, :] = hidden.astype(BF16)
+            give_hidden(c, core, core)
+        for side in (0, 1):
+            give_hidden(c, side, 1 - side)
+
+    def hidden_rows(c, rel, core):
+        r0, count = chunk_rows(c)
+        return hb.at[rel, core, pl.ds(r0, count)]
+
+    def give_hidden(c, side, core):
+        sem = hr_sem.at[c, side if core == side else 2 + side]
+        remote(hidden_rows(c, 0, core), hidden_rows(c, 1 + 2 * side, core), hs_sem, sem, sides[side])
 
     def next_hidden(c):
-        r0, count = chunk_rows(c)
-        for side in (0, 1):
-            handles["h", c, side].wait_recv()
-            rows = pl.ds(r0 + side * (count // 2), count // 2)
-            handles["k", c, side] = remote(
-                hb.at[1 + 2 * side, rows],
-                hb.at[2, rows],
-                hs_sem,
-                hr_sem.at[c, 2],
-                sides[side],
-            )
+        for side in (0, 1):
+            block = hidden_rows(c, 1 + 2 * side, side)
+            arrived(block, hr_sem.at[c, side])
+            remote(block, hidden_rows(c, 2, side), hs_sem, hr_sem.at[c, 4], sides[side])
 
     def second_product(c):
         r0, count = chunk_rows(c)
-        arrived(hb.at[2, pl.ds(r0, count)], hr_sem.at[c, 2])
+        for side in (0, 1):
+            arrived(hidden_rows(c, 1 + 2 * side, 1 - side), hr_sem.at[c, 2 + side])
+        arrived(hb.at[2, :, pl.ds(r0, count)], hr_sem.at[c, 4])
         total = None
         for rel in range(YN):
             first = pl.multiple_of(origin[rel] * units, units)
             for core in range(CN):
                 term = jnp.dot(
-                    hb[rel, r0 : r0 + count, core * units : (core + 1) * units],
+                    hb[rel, core, r0 : r0 + count, :],
                     wdv[core, pl.ds(first, units), :],
                     preferred_element_type=F32,
                 )
@@ -346,12 +347,15 @@
     dma = pltpu.SemaphoreType.DMA
     scratch = [
         pltpu.VMEM((row_count, width), BF16),
-        dma(()),
+        pltpu.VMEM((1, width), F32),
+        pltpu.VMEM((2, row_count), jnp.int32),
+        pltpu.VMEM((2, row_count), F32),
+        dma((4,)),
         pltpu.VMEM((messages * K3, pieces, 128), BF16),
         pltpu.VMEM((2, YN, messages * K3, pieces, 128), BF16),
         pltpu.VMEM((max(2 * most * CAP, messages * K3) * pieces, 128), F32),
         pltpu.VMEM((2 * most * CAP, width), BF16),
-        pltpu.VMEM((YN, 2 * rows, CN * units), BF16),
+        pltpu.VMEM((YN, CN, 2 * rows, units), BF16),
         pltpu.VMEM((CN, width, units), BF16),
         pltpu.VMEM((CN, width, units), BF16),
         pltpu.VMEM((CN, block, columns), BF16),
@@ -368,11 +372,11 @@
         dma(()),
         dma((n,)),
         dma(()),
-        dma((n, 3)),
+        dma((n, 5)),
         dma(()),
         dma((n,)),
         dma(()),
-        dma((n, 3)),
+        dma((n, 5)),
         dma(()),
         dma((n,)),
         dma(()),
@@ -383,7 +387,7 @@
     return pl.pallas_call(
         functools.partial(kernel, zn),
         out_shape=jax.ShapeDtypeStruct((row_count, columns), BF16),
-        in_specs=[hbm, vmem, vmem, vmem, hbm, hbm, hbm],
+        in_specs=[hbm] * 7,
         out_specs=vmem,
         scratch_shapes=scratch,
         compiler_params=pltpu.CompilerParams(

time: 87.5 us -> 85.6 us (0.978)
  Pallas kernels: 85.7 us -> 83.9 us
    pallas_call x1, Pallas kernels: 85.7 us -> 83.9 us  [on_device(): pl.pallas_call(functools.partial(kernel, zn), out_shape=jax.ShapeDtypeStr...]
where the time goes in v4:
time: 85.6 us; the launch traced here: 85.5 us
  Pallas kernels  83.9 us (98%)
  local copies, waits for them, and re-layouts  1.57 us (2%)
    pallas_call x1, Pallas kernels, on_device(): pl.pallas_call(functools.partial(kernel, zn), out_shape=jax.ShapeDtypeStr...  83.9 us

profile of v4, /device:TPU:1, one launch (start us, length us, event | category | flops | bytes accessed | tf_op | source)
XLA Modules:
  0.0 85.5 jit_solution(18126265289034047969)
XLA Ops:
  0.0 83.9 %expert_layer.1 = bf16[128,512]{1,0:T(8,128)(2,1)} custom-call(bf16[128,2048]{1,0:T(8,128)(2,1)} %tokens_hbm.1, f32[1,2048]{1,0:T(1,128)} %bitcast.3, s32[2,128]{1,0:T(2,128)} %bitcast.4, f32[2,128]{1,0:T(2,128)} %bitcast.5, bf16[2048,256]{1,0:T(8,128)(2,1)} %w_gate.1, bf16[2048,256]{1,0:T(8,128)(2,1)} %w_up.1, bf16[1024,512]{1,0:T(8,128)(2,1)} %w_down.1), custom_call_target="tpu_custom_call" | custom-call | tf_op jit(solution)/shard_map/expert_layer/pallas_call | solution.py:387
  83.9 1.6 %copy.9 = bf16[128,512]{1,0:T(8,128)(2,1)} copy(bf16[128,512]{1,0:T(8,128)(2,1)} %expert_layer.1) | data formatting | bytes 262144

commit v5 on v4

--- a/solution.py
+++ b/solution.py
@@ -353,7 +353,7 @@
         dma((4,)),
         pltpu.VMEM((messages * K3, pieces, 128), BF16),
         pltpu.VMEM((2, YN, messages * K3, pieces, 128), BF16),
-        pltpu.VMEM((max(2 * most * CAP, messages * K3) * pieces, 128), F32),
+        pltpu.VMEM((max(2 * most * CAP, messages * K3) * pieces + pieces, 128), F32),
         pltpu.VMEM((2 * most * CAP, width), BF16),
         pltpu.VMEM((YN, CN, 2 * rows, units), BF16),
         pltpu.VMEM((CN, width, units), BF16),
@@ -362,7 +362,7 @@
         pltpu.VMEM((rows, columns), F32),
         pltpu.VMEM((rows, columns), BF16),
         pltpu.VMEM((rows, columns), BF16),
-        pltpu.VMEM((rows * out_pieces, 128), F32),
+        pltpu.VMEM((rows * out_pieces + 8, 128), F32),
         pltpu.VMEM((rows * out_pieces, 128), BF16),
         pltpu.VMEM((rows * out_pieces, 128), BF16),
         pltpu.VMEM((rows, columns), BF16),

time: 85.6 us -> 85.6 us (level)
  no operation moved by 1% of the time
where the time goes in v5:
time: 85.6 us; the launch traced here: 85.4 us
  Pallas kernels  83.9 us (98%)
  local copies, waits for them, and re-layouts  1.57 us (2%)
    pallas_call x1, Pallas kernels, on_device(): pl.pallas_call(functools.partial(kernel, zn), out_shape=jax.ShapeDtypeStr...  83.9 us

profile of v5, /device:TPU:1, one launch (start us, length us, event | category | flops | bytes accessed | tf_op | source)
XLA Modules:
  0.0 85.4 jit_solution(10372344128669819493)
XLA Ops:
  0.0 83.9 %expert_layer.1 = bf16[128,512]{1,0:T(8,128)(2,1)} custom-call(bf16[128,2048]{1,0:T(8,128)(2,1)} %tokens_hbm.1, f32[1,2048]{1,0:T(1,128)} %bitcast.3, s32[2,128]{1,0:T(2,128)} %bitcast.4, f32[2,128]{1,0:T(2,128)} %bitcast.5, bf16[2048,256]{1,0:T(8,128)(2,1)} %w_gate.1, bf16[2048,256]{1,0:T(8,128)(2,1)} %w_up.1, bf16[1024,512]{1,0:T(8,128)(2,1)} %w_down.1), custom_call_target="tpu_custom_call" | custom-call | tf_op jit(solution)/shard_map/expert_layer/pallas_call | solution.py:387
  83.9 1.6 %copy.9 = bf16[128,512]{1,0:T(8,128)(2,1)} copy(bf16[128,512]{1,0:T(8,128)(2,1)} %expert_layer.1) | data formatting | bytes 262144
